TPU v7x, 512 devices: a whole 4x4x16 slice. The times are simulated.
512 devices in a mesh: ep: 32 (over z, core), tp: 16 (over y, x).
Axes of the slice: x: 4, y: 4, z: 16, core: 2. Of those that a mesh axis runs over, the one named last changes fastest.
Arguments:
- query_rows: bfloat16 [16384, 2048], P('ep', 'tp'), may hold values from -6 to 6
- key_rows: bfloat16 [16384, 2048], P('ep', 'tp'), may hold values from -6 to 6
- value_rows: bfloat16 [16384, 4096], P('ep', 'tp'), may hold values from -6 to 6
- in_gate: float32 [16, 16384], P('tp', 'ep'), may hold values from -120 to 120
- forget_gate: float32 [16, 16384], P('tp', 'ep'), may hold values from -2 to 20
- out_gate: bfloat16 [16384, 4096], P('ep', 'tp'), may hold values from -6 to 6
- head_gain: float32 [4096], P('tp'), may hold values from 0.1 to 1.9
- mix_weight: bfloat16 [4096, 4096], P(None, 'tp'), may hold values from -0.09375 to 0.09375
- expert_input: bfloat16 [8192, 4096], P('ep', 'tp'), may hold values from -30 to 30
- routes: int32 [8192, 2], P('ep'), may hold values from 0 to 31, all different within a row; in each aligned block of 256 rows (0 to 255, 256 to 511, ...) at most 32 rows name the same one
- route_weight: float32 [8192, 2], P('ep'), may hold values from 0.25 to 1.25
- gate_weight: bfloat16 [32, 1024, 4096], P('ep', 'tp'), may hold values from -0.09375 to 0.09375
- up_weight: bfloat16 [32, 1024, 4096], P('ep', 'tp'), may hold values from -0.09375 to 0.09375
- down_weight: bfloat16 [32, 1024, 4096], P('ep', None, 'tp'), may hold values from -0.1875 to 0.1875
Outputs:
- mixer_out: bfloat16 [16384, 4096], P('ep', 'tp')
- expert_out: bfloat16 [8192, 4096], P('ep', 'tp')
Inputs may be any that keep to these rules, and one draw needn't show every extreme that they name: `routes`: each row names 2 different experts. In the rows of one device no expert is named by more than 32 rows, and in the rows of some device an expert is named by exactly 32 rows.
All inputs are finite; a program needn't handle non-finite values.
Results may differ from a plain program's by a relative error of at most 0.0057.
Values may be sent and summed in bfloat16 or wider, within the bound.
No kernel may reach another device: no remote copies, remote signals or barrier semaphores. Data moves between devices by JAX's collectives and lax.ppermute only.
A program may use at most 128 MiB of HBM per device.

v0:
```python
import jax
import jax.numpy as jnp
from jax import lax
from jax.sharding import Mesh
from jax.sharding import PartitionSpec as P

D = 4096
BLOCK = 64
EP = ("ep_0", "ep_1")
EPSILON = 1e-06
LOG_FLOOR = -1e30
HIGHEST_PRECISION = lax.Precision.HIGHEST


def nothing_yet(x, identity):
    return jax.tree.map(
        lambda part, zero: jnp.zeros_like(part) + jnp.asarray(zero, part.dtype), x, identity
    )


def collected_together(x, axis):
    leaves = jax.tree.leaves(x)
    turns = sorted(range(len(leaves)), key=lambda k: -leaves[k].size)
    width = (1, *leaves[turns[0]].shape)[-1]
    lines = [
        jnp.pad(leaves[k].reshape(-1), (0, -leaves[k].size % width)).reshape(-1, width)
        for k in turns
    ]
    both, at, found = (lax.all_gather(jnp.concatenate(lines), axis), 0, {})
    for k, line in zip(turns, lines):
        share = both[:, at : at + len(line)].reshape(len(both), -1)
        found[k] = share[:, : leaves[k].size].reshape(-1, *leaves[k].shape)
        at += len(line)
    numbers = iter(range(len(leaves)))
    return jax.tree.map(lambda _: found[next(numbers)], x)


def prefix_by_axis(x, axes, combine, identity):
    before = start = nothing_yet(x, identity)
    subtotal = x
    for axis in reversed(axes):
        length, index = (lax.axis_size(axis), lax.axis_index(axis))
        pieces = collected_together(subtotal, axis)
        inside, subtotal = (start, start)
        for k in range(length):
            passed = k < index
            subtotal = combine(subtotal, jax.tree.map(lambda part: part[k], pieces))
            inside = jax.tree.map(lambda new, old: jnp.where(passed, new, old), subtotal, inside)
        before = combine(inside, before)
    return before


def joined_along(tiles, dim):
    dims = list(tiles.shape[1:])
    dims[dim] *= tiles.shape[0]
    return jnp.moveaxis(tiles, 0, dim).reshape(dims)


def copy_for_each(x, axis):
    copies = jnp.broadcast_to(x, (lax.axis_size(axis), *x.shape))
    return lax.all_to_all(copies, axis, split_axis=0, concat_axis=0, tiled=True)


def gather_directly(x, axis, dim):
    return joined_along(copy_for_each(x, axis), dim)


def combine(first_part, second_part):
    decay_first, max_first, memory_first, normal_first = first_part
    decay_second, max_second, memory_second, normal_second = second_part
    running_max = jnp.maximum(decay_second + max_first, max_second)
    keep_first = jnp.exp(decay_second + max_first - running_max)
    keep_second = jnp.exp(max_second - running_max)
    memory = (
        keep_first[..., None, None] * memory_first + keep_second[..., None, None] * memory_second
    )
    normalizer = keep_first[..., None] * normal_first + keep_second[..., None] * normal_second
    return (decay_first + decay_second, running_max, memory, normalizer)


def identity_state(head_count, key_width, value_width):
    return (
        jnp.zeros((head_count,), jnp.float32),
        jnp.full((head_count,), LOG_FLOOR, jnp.float32),
        jnp.zeros((head_count, key_width, value_width), jnp.float32),
        jnp.zeros((head_count, key_width), jnp.float32),
    )


def halfprod(form, left, right):
    return jnp.einsum(form, left, right, preferred_element_type=jnp.float32)


def prepare(query_heads, key_heads, value_heads, in_gate, forget_gate):
    head_count, length, key_width = query_heads.shape
    block_count = length // BLOCK
    query_blocks = query_heads.reshape(head_count, block_count, BLOCK, key_width)
    key_blocks = key_heads.reshape(head_count, block_count, BLOCK, key_width)
    value_blocks = value_heads.reshape(head_count, block_count, BLOCK, value_heads.shape[-1])
    log_input = in_gate.reshape(head_count, block_count, BLOCK)
    cumulative = jnp.cumsum(
        jax.nn.log_sigmoid(forget_gate).reshape(head_count, block_count, BLOCK), axis=-1
    )
    block_decay = cumulative[..., -1]
    weight_log = block_decay[..., None] - cumulative + log_input
    block_max = jnp.max(weight_log, axis=-1)
    weighted = (
        key_blocks.astype(jnp.float32) * jnp.exp(weight_log - block_max[..., None])[..., None]
    )
    normalizer = jnp.sum(weighted, axis=2)
    memory = halfprod("hcsk,hcsv->hckv", weighted.astype(jnp.bfloat16), value_blocks)
    return (
        (query_blocks, key_blocks, value_blocks, log_input, cumulative),
        (block_decay, block_max, memory, normalizer),
    )


def prefix(summary, initial):
    leading = jax.tree.map(lambda tensor: jnp.moveaxis(tensor, 1, 0), summary)

    def advance(running, current):
        return (combine(running, current), running)

    final_state, before = lax.scan(advance, initial, leading)
    return (final_state, jax.tree.map(lambda tensor: jnp.moveaxis(tensor, 0, 1), before))


def block_outputs(blocked, before):
    query_blocks, key_blocks, value_blocks, log_input, cumulative = blocked
    prior_max, prior_memory, prior_normal = (before[1], before[2], before[3])
    block_len = cumulative.shape[-1]
    scale = query_blocks.shape[-1] ** (-0.5)
    causal = jnp.tril(jnp.ones((block_len, block_len), dtype=bool))
    log_decay = jnp.where(
        causal,
        cumulative[..., :, None] - cumulative[..., None, :] + log_input[..., None, :],
        -jnp.inf,
    )
    log_inter = cumulative + prior_max[..., None]
    top_value = jnp.maximum(log_inter, jnp.max(log_decay, axis=-1))
    scores = (
        halfprod("hctk,hcsk->hcts", query_blocks, key_blocks)
        * scale
        * jnp.exp(log_decay - top_value[..., None])
    )
    carried = jnp.exp(log_inter - top_value) * scale
    query_wide = query_blocks.astype(jnp.float32)
    numerator = carried[..., None] * jnp.einsum(
        "hctk,hckv->hctv", query_wide, prior_memory, precision=HIGHEST_PRECISION
    ) + halfprod("hcts,hcsv->hctv", scores.astype(jnp.bfloat16), value_blocks)
    denominator = carried * jnp.einsum(
        "hctk,hck->hct", query_wide, prior_normal, precision=HIGHEST_PRECISION
    ) + jnp.sum(scores, axis=-1)
    return numerator / jnp.maximum(jnp.abs(denominator), jnp.exp(-top_value))[..., None]


def finish(head_values, out_gate, head_gain):
    head_count, block_count, block_len, value_width = head_values.shape
    per_head = jnp.transpose(head_values, (1, 2, 0, 3)).reshape(
        block_count * block_len, head_count, value_width
    )
    per_head = per_head * lax.rsqrt(jnp.mean(per_head * per_head, axis=-1, keepdims=True) + EPSILON)
    per_head = per_head.reshape(block_count * block_len, head_count * value_width) * head_gain
    per_head = per_head * jax.nn.sigmoid(out_gate.astype(jnp.float32))
    return per_head.astype(jnp.bfloat16)


def cell_heads(query_rows, key_rows, value_rows, in_gate, forget_gate, out_gate, head_gain):
    length = query_rows.shape[0]
    head_count = in_gate.shape[0]
    key_width = query_rows.shape[1] // head_count
    value_width = value_rows.shape[1] // head_count
    query_heads = query_rows.reshape(length, head_count, key_width).transpose(1, 0, 2)
    key_heads = key_rows.reshape(length, head_count, key_width).transpose(1, 0, 2)
    value_heads = value_rows.reshape(length, head_count, value_width).transpose(1, 0, 2)
    blocked, summary = prepare(query_heads, key_heads, value_heads, in_gate, forget_gate)
    initial = identity_state(head_count, key_width, value_width)
    final_state, before = prefix(summary, initial)
    incoming = prefix_by_axis(final_state, EP, combine, initial)
    expanded = jax.tree.map(lambda tensor: tensor[:, None], incoming)
    before = combine(expanded, before)
    return finish(block_outputs(blocked, before), out_gate, head_gain)


def body(
    query_rows,
    key_rows,
    value_rows,
    in_gate,
    forget_gate,
    out_gate,
    head_gain,
    mix_weight,
    expert_input,
    routes,
    route_weight,
    gate_weight,
    up_weight,
    down_weight,
):
    mixed_heads = cell_heads(
        query_rows, key_rows, value_rows, in_gate, forget_gate, out_gate, head_gain
    )
    gate_local = gate_weight[0]
    up_local = up_weight[0]
    down_local = down_weight[0]
    group_size = lax.axis_size(EP)
    token_count, fanout = routes.shape
    capacity = 2 * token_count * fanout // group_size
    slot_count = group_size * capacity
    chosen = routes.reshape(-1)
    one_hot = (chosen[:, None] == jnp.arange(group_size, dtype=jnp.int32)[None, :]).astype(
        jnp.int32
    )
    position = jnp.sum((jnp.cumsum(one_hot, axis=0) - one_hot) * one_hot, axis=1)
    target = chosen * capacity + position
    matches = (jnp.arange(slot_count, dtype=jnp.int32)[:, None] == target[None, :]).astype(
        jnp.int32
    )
    occupied = jnp.sum(matches, axis=1) > 0
    source_row = jnp.sum(
        matches * (jnp.arange(token_count * fanout, dtype=jnp.int32) // fanout)[None, :], axis=1
    )
    arrived = lax.all_to_all(
        jnp.where(
            occupied[:, None],
            jnp.take(expert_input, source_row, axis=0),
            jnp.zeros((), expert_input.dtype),
        ),
        EP,
        split_axis=0,
        concat_axis=0,
        tiled=True,
    )
    head_piece = lax.all_gather(mixed_heads, "tp", axis=1, tiled=True)
    token_piece = lax.all_gather(arrived, "tp", axis=1, tiled=True)
    mix_acc = jnp.dot(head_piece, mix_weight, preferred_element_type=jnp.float32)
    gate_acc = jnp.einsum("sd,fd->sf", token_piece, gate_local, preferred_element_type=jnp.float32)
    up_acc = jnp.einsum("sd,fd->sf", token_piece, up_local, preferred_element_type=jnp.float32)
    squares = jnp.sum(jnp.square(token_piece.astype(jnp.float32)), axis=1)
    mix_acc, gate_acc, up_acc, squares = (mix_acc, gate_acc, up_acc, squares)
    mixer_out = mix_acc.astype(jnp.bfloat16)
    inverse_rms = lax.rsqrt(squares / D + EPSILON)[:, None]
    hidden = (jax.nn.silu(gate_acc * inverse_rms) * (up_acc * inverse_rms)).astype(jnp.bfloat16)
    expert_rows = jnp.dot(
        gather_directly(hidden, "tp", 1), down_local, preferred_element_type=jnp.float32
    )
    returned_rows = lax.all_to_all(
        expert_rows.astype(jnp.bfloat16), EP, split_axis=0, concat_axis=0, tiled=True
    )
    picked_rows = (
        jnp.take(returned_rows, target, axis=0).reshape(token_count, fanout, -1).astype(jnp.float32)
    )
    expert_out = jnp.sum(picked_rows * route_weight[:, :, None], axis=1).astype(jnp.bfloat16)
    return (mixer_out, expert_out)


def solution(mesh):
    split = Mesh(mesh.devices.reshape(16, 2, mesh.shape["tp"]), ("ep_0", "ep_1", "tp"))
    in_specs = (
        P(EP, "tp"),
        P(EP, "tp"),
        P(EP, "tp"),
        P("tp", EP),
        P("tp", EP),
        P(EP, "tp"),
        P("tp"),
        P(None, "tp"),
        P(EP, "tp"),
        P(EP, None),
        P(EP, None),
        P(EP, "tp", None),
        P(EP, "tp", None),
        P(EP, None, "tp"),
    )
    out_specs = (P(EP, "tp"), P(EP, "tp"))
    return jax.shard_map(body, mesh=split, in_specs=in_specs, out_specs=out_specs, check_vma=False)
```

profile of v0, /device:TPU:1, one launch (start us, length us, event | category | flops | bytes accessed | tf_op | source)
XLA Modules:
  0.0 352.5 jit_solution(5622983685871281707)
XLA Ops:
  7.3 0.8 fusion.55
  8.6 0.5 broadcast.772
  9.1 1.3 reduce.22
  10.6 0.8 reshape.1181
  11.6 1.1 fusion.21
  12.6 1.5 convolution_bitcast_fusion
  14.2 36.5 %while.25 = (s32[]{:T(128)}, f32[1]{0:T(128)}, f32[1]{0:T(128)}, f32[1,128,256]{2,1,0:T(8,128)S(1)}, f32[1,128]{1,0:T(1,128)S(1)}, /*index=5*/f32[8,1]{0,1:T(1,1...) while((s32[]{:T(128)}, f32[1]{0:T(128)}, f32[1]{0:T(128)}, ...), condition=%wide.region_4.5_spmd.clone, body=%wide.region_3.4_spmd.clone.sunk | while | flops 164488 | bytes 659258 | solution.py:124
  14.2 0.6 constant_dynamic-slice_fusion.4
  16.7 0.7 bitcast_dynamic-update-slice_fusion.2
  17.4 0.6 constant_dynamic-update-slice_fusion.2
  18.7 0.6 constant_dynamic-slice_fusion.4
  21.2 0.7 bitcast_dynamic-update-slice_fusion.2
  21.9 0.6 constant_dynamic-update-slice_fusion.2
  23.2 0.6 constant_dynamic-slice_fusion.4
  25.7 0.7 bitcast_dynamic-update-slice_fusion.2
  26.5 0.6 constant_dynamic-update-slice_fusion.2
  27.8 0.6 constant_dynamic-slice_fusion.4
  30.3 0.7 bitcast_dynamic-update-slice_fusion.2
  31.1 0.6 constant_dynamic-update-slice_fusion.2
  32.4 0.6 constant_dynamic-slice_fusion.4
  34.9 0.7 bitcast_dynamic-update-slice_fusion.2
  35.7 0.6 constant_dynamic-update-slice_fusion.2
  37.0 0.6 constant_dynamic-slice_fusion.4
  39.5 0.7 bitcast_dynamic-update-slice_fusion.2
  40.2 0.5 constant_dynamic-update-slice_fusion.2
  41.5 0.6 constant_dynamic-slice_fusion.4
  44.0 0.7 bitcast_dynamic-update-slice_fusion.2
  44.7 0.5 constant_dynamic-update-slice_fusion.2
  46.0 0.6 constant_dynamic-slice_fusion.4
  48.5 0.7 bitcast_dynamic-update-slice_fusion.2
  49.2 0.6 constant_dynamic-update-slice_fusion.2
  50.7 0.5 copy-done.15
  51.2 8.5 %all-gather.2 = f32[2,131,256]{2,1,0:T(8,128)S(1)} all-gather(f32[1,131,256]{2,1,0:T(8,128)S(1)} %maximum_bitcast_fusion), channel_id=2, replica_groups=mesh['ep_0'=16,'ep_1'=2,'tp'=16] {'ep_1'}, dimensions={0}, use_global_device_ids=true | all-gather | bytes 402432 | tf_op jit(solution)/shard_map/all_gather | solution.py:29
  59.7 0.6 fusion.86
  60.3 0.5 fusion.87
  66.3 0.7 maximum_bitcast_fusion.1
  67.0 0.8 copy.54
  68.1 1.2 reduce-window.6
  69.7 0.6 convert_reduce_fusion
  70.5 3.9 %gather_fusion = bf16[1024,256]{1,0:T(8,128)(2,1)S(1)} fusion(bf16[256,256]{1,0:T(8,128)(2,1)S(1)} %copy-done.1, s32[1024]{0:T(1024)S(1)} %broadcast_clamp_fusion), kind=kCustom, calls=%fused_computation | custom fusion | bytes 1052672 | tf_op jit(solution)/shard_map/jit(_take)/gather | solution.py:227
  74.6 0.3 select_select_fusion
  74.9 48.4 %all_to_all.26 = bf16[32,32,256]{2,1,0:T(8,128)(2,1)} all-to-all(bf16[32,32,256]{2,1,0:T(8,128)(2,1)S(1)} %select_select_fusion), channel_id=1, replica_groups=mesh['ep_0'=16,'ep_1'=2,'tp'=16] {'ep_0','ep_1'}, dimensions={0} | all-to-all | bytes 1048576 | tf_op jit(solution)/shard_map/all_to_all | solution.py:224
  124.7 22.1 %all-gather.12.cloned.1.call-done = f32[16,131,256]{2,1,0:T(8,128)} async-done(((f32[1,131,256]{2,1,0:T(8,128)}), f32[16,131,256]{2,1,0:T(8,128)}) %all-gather.12.cloned.1.call-update) | async-done | bytes 2146320 | tf_op jit(solution)/shard_map/all_gather | solution.py:29
  146.8 1.1 fusion.82
  147.9 0.7 fusion.85
  149.2 0.6 fusion.84
  180.3 0.3 fusion.89
  181.0 2.0 fusion.26
  183.0 0.3 fusion.44
  183.3 0.8 multiply_reduce_fusion.2
  184.2 0.9 fusion.17
  185.1 59.3 %all-gather.10.cloned.1.call-done = bf16[1024,4096]{1,0:T(8,128)(2,1)} async-done(((bf16[1024,256]{1,0:T(8,128)(2,1)}), bf16[1024,4096]{1,0:T(8,128)(2,1)}) %all-gather.10.cloned.1.call-update) | async-done | bytes 8388624 | tf_op jit(solution)/shard_map/all_gather | solution.py:236
  244.4 5.2 %multiply_reduce_fusion = f32[1024]{0:T(1024)S(1)} fusion(bf16[1024,4096]{1,0:T(8,128)(2,1)} %all-gather.10.cloned.1.call-done), kind=kLoop, calls=%fused_computation.12 | loop fusion | flops 12581888 | bytes 8392704 | tf_op jit(solution)/shard_map/reduce_sum | solution.py:240
  249.6 0.5 copy-done.2
  250.1 2.7 convolution_multiply_fusion.3
  252.8 2.7 fusion.8
  255.8 35.5 %all_to_all.27 = bf16[16,1024,64]{1,2,0:T(8,128)(2,1)S(1)} all-to-all(bf16[16,1024,64]{1,2,0:T(8,128)(2,1)S(1)} %broadcast_in_dim.75), channel_id=1, replica_groups=mesh['ep_0'=16,'ep_1'=2,'tp'=16] {'tp'}, dimensions={0} | all-to-all | bytes 4194304 | tf_op jit(solution)/shard_map/all_to_all | solution.py:61
  291.3 1.6 convolution_convert_fusion
  292.9 15.3 %all-to-all-start.2 = ((bf16[32,32,256]{2,1,0:T(8,128)(2,1)}), bf16[32,32,256]{2,1,0:T(8,128)(2,1)S(1)}, u32[]{:S(2)}, u32[]{:S(2)}) async-start(bf16[32,32,256]{2,1,0:T(8,128)(2,1)} %bitcast.139), calls=%async_computation.2 | async-start | bytes 1048576 | tf_op jit(solution)/shard_map/all_to_all | solution.py:248
  309.1 22.7 %all-gather.8.cloned.1.call-done = bf16[512,4096]{1,0:T(8,128)(2,1)} async-done(((bf16[512,256]{1,0:T(8,128)(2,1)}), bf16[512,4096]{1,0:T(8,128)(2,1)}) %all-gather.8.cloned.1.call-update) | async-done | bytes 4194320 | tf_op jit(solution)/shard_map/all_gather | solution.py:235
  331.8 4.1 %convolution_convert_fusion.1 = bf16[512,256]{1,0:T(8,128)(2,1)} fusion(bf16[512,4096]{1,0:T(8,128)(2,1)} %all-gather.8.cloned.1.call-done, bf16[4096,256]{1,0:T(8,128)(2,1)S(1)} %copy-done), kind=kOutput, calls=%fused_computation.22 | convolution fusion | flops 1073872896 | bytes 6553600 | tf_op jit(solution)/shard_map/dot_general | solution.py:237
  335.9 5.8 %all-to-all-done.2 = bf16[32,32,256]{2,1,0:T(8,128)(2,1)S(1)} async-done(((bf16[32,32,256]{2,1,0:T(8,128)(2,1)}), bf16[32,32,256]{2,1,0:T(8,128)(2,1)S(1)}, u32[]{:S(2)}, u32[]{:S(2)}) %all-to-all-start.2) | async-done | bytes 524320 | tf_op jit(solution)/shard_map/all_to_all | solution.py:248
  341.7 1.9 gather_fusion.1
  343.8 2.2 multiply_reduce_fusion.1
  (150 shorter events, 6.6 us)
Async XLA Ops:
  7.2 324.6 %copy-start = (bf16[4096,256]{1,0:T(8,128)(2,1)S(1)}, bf16[4096,256]{1,0:T(8,128)(2,1)}, u32[]{:S(2)}) copy-start(bf16[4096,256]{1,0:T(8,128)(2,1)} %param.23) | copy-start | bytes 6291460
  7.2 139.6 %all-gather.12.cloned.1.call-start = ((), (), s32[]{:S(2)}) async-start(), calls=%async_computation.5 | async-start | bytes 2367488 | tf_op jit(solution)/shard_map/all_gather | solution.py:29
  8.4 5.7 %copy-start.7 = (f32[1,8,64]{2,1,0:T(8,128)}, f32[1,8,64]{2,1,0:T(8,128)S(1)}, u32[]{:S(2)}) copy-start(f32[1,8,64]{2,1,0:T(8,128)S(1)} %reduce_window_sum.28) | copy-start | bytes 6148
  11.3 2.8 copy-start.9
  14.1 56.4 %copy-start.1 = (bf16[256,256]{1,0:T(8,128)(2,1)S(1)}, bf16[256,256]{1,0:T(8,128)(2,1)}, u32[]{:S(2)}) copy-start(bf16[256,256]{1,0:T(8,128)(2,1)} %param.24) | copy-start | bytes 393220
  50.6 0.5 copy-start.15
  50.6 0.6 copy-start.17
  67.0 177.4 %all-gather.10.cloned.1.call-start = ((), (), s32[]{:S(2)}) async-start(), calls=%async_computation.4 | async-start | bytes 8912896 | tf_op jit(solution)/shard_map/all_gather | solution.py:236
  74.5 49.9 %copy-start.8 = (f32[1,8,64]{2,1,0:T(8,128)S(1)}, f32[1,8,64]{2,1,0:T(8,128)}, u32[]{:S(2)}) copy-start(f32[1,8,64]{2,1,0:T(8,128)} %copy-done.7) | copy-start | bytes 6148
  74.5 49.9 %copy-start.10 = (f32[8,64]{1,0:T(8,128)S(1)}, f32[8,64]{1,0:T(8,128)}, u32[]{:S(2)}) copy-start(f32[8,64]{1,0:T(8,128)} %copy-done.9) | copy-start | bytes 6148
  74.5 105.5 %copy-start.16 = (f32[8,1]{0,1:T(1,128)S(1)}, f32[8,1]{0,1:T(1,128)}, u32[]{:S(2)}) copy-start(f32[8,1]{0,1:T(1,128)} %copy-done.15) | copy-start | bytes 100
  74.5 105.5 %copy-start.18 = (f32[8,1]{0,1:T(1,128)S(1)}, f32[8,1]{0,1:T(1,128)}, u32[]{:S(2)}) copy-start(f32[8,1]{0,1:T(1,128)} %copy-done.17) | copy-start | bytes 100
  74.5 105.7 %copy-start.12 = (f32[8,1,128]{2,1,0:T(1,128)S(1)}, f32[8,1,128]{2,1,0:T(1,128)}, u32[]{:S(2)}) copy-start(f32[8,1,128]{2,1,0:T(1,128)} %get-tuple-element.83) | copy-start | bytes 12292
  74.5 105.8 %copy-start.22 = (bf16[512,128]{1,0:T(8,128)(2,1)S(1)}, bf16[512,128]{1,0:T(8,128)(2,1)}, u32[]{:S(2)}) copy-start(bf16[512,128]{1,0:T(8,128)(2,1)} %param.16) | copy-start | bytes 393220
  74.5 106.1 %copy-start.5 = (bf16[512,128]{1,0:T(8,128)(2,1)S(1)}, bf16[512,128]{1,0:T(8,128)(2,1)}, u32[]{:S(2)}) copy-start(bf16[512,128]{1,0:T(8,128)(2,1)} %param.17) | copy-start | bytes 393220
  123.3 59.7 %copy-start.3 = (bf16[512,256]{1,0:T(8,128)(2,1)S(1)}, bf16[512,256]{1,0:T(8,128)(2,1)}, u32[]{:S(2)}) copy-start(bf16[512,256]{1,0:T(8,128)(2,1)} %param.18) | copy-start | bytes 786436
  123.3 208.4 %all-gather.8.cloned.1.call-start = ((), (), s32[]{:S(2)}) async-start(), calls=%async_computation.3 | async-start | bytes 4456448 | tf_op jit(solution)/shard_map/all_gather | solution.py:235
  180.3 3.0 copy-start.19
  180.3 3.0 copy-start.23
  183.0 1.2 copy-start.6
  183.0 1.2 copy-start.14
  184.2 65.4 %copy-start.4 = (bf16[1,64,4096]{2,1,0:T(8,128)(2,1)S(1)}, bf16[1,64,4096]{2,1,0:T(8,128)(2,1)}, u32[]{:S(2)}) copy-start(bf16[1,64,4096]{2,1,0:T(8,128)(2,1)} %param.27) | copy-start | bytes 1572868
  244.4 5.8 %copy-start.2 = (bf16[1024,4096]{1,0:T(8,128)(2,1)S(1)}, bf16[1024,4096]{1,0:T(8,128)(2,1)}, u32[]{:S(2)}) copy-start(bf16[1024,4096]{1,0:T(8,128)(2,1)} %all-gather.10.cloned.1.call-done) | copy-start | bytes 25165828
  250.1 2.7 copy-start.20
  255.8 35.5 %copy-start.21 = (bf16[1,1024,256]{2,1,0:T(8,128)(2,1)S(1)}, bf16[1,1024,256]{2,1,0:T(8,128)(2,1)}, u32[]{:S(2)}) copy-start(bf16[1,1024,256]{2,1,0:T(8,128)(2,1)} %param.29) | copy-start | bytes 1572868
  291.3 17.0 %copy-start.11 = (s32[256,2]{0,1:T(2,128)S(1)}, s32[256,2]{0,1:T(2,128)}, u32[]{:S(2)}) copy-start(s32[256,2]{0,1:T(2,128)} %param.25) | copy-start | bytes 6148
  291.3 17.6 %copy-start.13 = (f32[256,2]{0,1:T(2,128)S(1)}, f32[256,2]{0,1:T(2,128)}, u32[]{:S(2)}) copy-start(f32[256,2]{0,1:T(2,128)} %param.26) | copy-start | bytes 6148
  292.9 48.8 %all-to-all-start.2 = ((bf16[32,32,256]{2,1,0:T(8,128)(2,1)}), bf16[32,32,256]{2,1,0:T(8,128)(2,1)S(1)}, u32[]{:S(2)}, u32[]{:S(2)}) async-start(bf16[32,32,256]{2,1,0:T(8,128)(2,1)} %bitcast.139), calls=%async_computation.2 | async-start | bytes 1048576 | tf_op jit(solution)/shard_map/all_to_all | solution.py:248
Sparse Core Ops, SparseCore 0:
  67.1 79.6 all-gather.11
  149.7 94.5 all-gather.9
  247.9 83.7 all-gather.7
where the time goes:
time: 354 us; the launch traced here: 352 us
  waiting for transfers between devices  110 us (31%)
  blocking collectives  92.4 us (26%)
  between operations  51.3 us (14%)
  other arithmetic  28 us (8%)
  local copies, waits for them, and re-layouts  21.5 us (6%)
  loops' own time  19.7 us (6%)
  starting transfers between devices  15.6 us (4%)
  matrix products  14.2 us (4%)
    all_gather x1, waiting for transfers between devices, body(): token_piece = lax.all_gather(arrived, 'tp', axis=1, tiled=True)  59.3 us
    all_to_all x1, blocking collectives, body(): lax.all_to_all(jnp.where(occupied[:, None], jnp.take(expert_input, source...  48.4 us
    all_to_all x1, blocking collectives, copy_for_each(): return lax.all_to_all(copies, axis, split_axis=0, concat_axis=0, tiled=True)  35.5 us
    all_gather x1, waiting for transfers between devices, body(): head_piece = lax.all_gather(mixed_heads, 'tp', axis=1, tiled=True)  22.7 us
    all_gather x1, waiting for transfers between devices, collected_together(): both, at, found = (lax.all_gather(jnp.concatenate(lines), axis), 0, {})  22.1 us
    another operation x1, loops' own time, prefix(): final_state, before = lax.scan(advance, initial, leading)  19.7 us
    all_to_all x1, starting transfers between devices, body(): lax.all_to_all(expert_rows.astype(jnp.bfloat16), EP, split_axis=0, concat...  15.3 us
    dynamic_update_slice x16, other arithmetic, prefix(): final_state, before = lax.scan(advance, initial, leading)  9.85 us
  transfers between devices with their start and end apart: 4, of which 4 were waited for; matrix products, arithmetic and copies ran while one was open for 9% of the time, Pallas kernels for 0%

commit v1 on v0

--- a/solution.py
+++ b/solution.py
@@ -1,3 +1,4 @@
+import functools
 import jax
 import jax.numpy as jnp
 from jax import lax
@@ -10,6 +11,14 @@
 EPSILON = 1e-06
 LOG_FLOOR = -1e30
 HIGHEST_PRECISION = lax.Precision.HIGHEST
+
+
+def run_the_shifts_all(t0, group_axis):
+    then = jnp.concatenate([t0 for _ in range(lax.axis_size(group_axis))], axis=1)
+    return lax.all_to_all(then, group_axis, 1, 1, tiled=True)
+
+
+state_the_figure = functools.partial(run_the_shifts_all, group_axis="tp")
 
 
 def nothing_yet(x, identity):
@@ -233,7 +242,7 @@
         tiled=True,
     )
     head_piece = lax.all_gather(mixed_heads, "tp", axis=1, tiled=True)
-    token_piece = lax.all_gather(arrived, "tp", axis=1, tiled=True)
+    token_piece = state_the_figure(arrived)
     mix_acc = jnp.dot(head_piece, mix_weight, preferred_element_type=jnp.float32)
     gate_acc = jnp.einsum("sd,fd->sf", token_piece, gate_local, preferred_element_type=jnp.float32)
     up_acc = jnp.einsum("sd,fd->sf", token_piece, up_local, preferred_element_type=jnp.float32)

time: 354 us -> 374 us (1.056)
  blocking collectives: 92.4 us -> 39.6 us
  local copies, waits for them, and re-layouts: 21.5 us -> 62.2 us
  starting transfers between devices: 15.6 us -> 37.6 us
  waiting for transfers between devices: 110 us -> 116 us
  other arithmetic: 28 us -> 31.9 us
    all_gather x1 -> x0, waiting for transfers between devices: 59.3 us -> none  [body(): token_piece = lax.all_gather(arrived, 'tp', axis=1, tiled=True)]
    all_to_all x1 -> x0, blocking collectives: 48.4 us -> none  [body(): lax.all_to_all(jnp.where(occupied[:, None], jnp.take(expert_input, source...]
    all_to_all x0 -> x2, waiting for transfers between devices: none -> 35.2 us  [the longest x1 35.2 us: run_the_shifts_all(): return lax.all_to_all(then, group_axis, 1, 1, tiled=True)]
    all_gather x1, waiting for transfers between devices: 22.1 us -> 52 us  [collected_together(): both, at, found = (lax.all_gather(jnp.concatenate(lines), axis), 0, {})]
    all_to_all x0 -> x2, starting transfers between devices: none -> 23.7 us  [the longest x1 16.8 us: body(): lax.all_to_all(jnp.where(occupied[:, None], jnp.take(expert_input, source...]
    all_gather x1, waiting for transfers between devices: 22.7 us -> 0.02 us  [body(): head_piece = lax.all_gather(mixed_heads, 'tp', axis=1, tiled=True)]
    all_to_all x1, waiting for transfers between devices: 5.79 us -> 28.4 us  [body(): lax.all_to_all(expert_rows.astype(jnp.bfloat16), EP, split_axis=0, concat...]
    dynamic_update_slice x16, local copies, waits for them, and re-layouts: 1.57 us -> 20.2 us  [prefix(): final_state, before = lax.scan(advance, initial, leading)]
  transfers between devices with their start and end apart: 4 -> 5, of which waited for: 4 -> 3; matrix products, arithmetic and copies ran while one was open for 9% -> 25% of each run, Pallas kernels for 0% -> 0%
where the time goes in v1:
time: 374 us; the launch traced here: 371 us
  waiting for transfers between devices  116 us (31%)
  local copies, waits for them, and re-layouts  62.2 us (17%)
  between operations  51.9 us (14%)
  blocking collectives  39.6 us (11%)
  starting transfers between devices  37.6 us (10%)
  other arithmetic  31.9 us (9%)
  loops' own time  19.9 us (5%)
  matrix products  11.9 us (3%)
    all_gather x1, waiting for transfers between devices, collected_together(): both, at, found = (lax.all_gather(jnp.concatenate(lines), axis), 0, {})  52 us
    all_to_all x1, blocking collectives, copy_for_each(): return lax.all_to_all(copies, axis, split_axis=0, concat_axis=0, tiled=True)  37.6 us
    all_to_all x1, waiting for transfers between devices, run_the_shifts_all(): return lax.all_to_all(then, group_axis, 1, 1, tiled=True)  35.2 us
    all_to_all x1, waiting for transfers between devices, body(): lax.all_to_all(expert_rows.astype(jnp.bfloat16), EP, split_axis=0, concat...  28.4 us
    dynamic_update_slice x16, local copies, waits for them, and re-layouts, prefix(): final_state, before = lax.scan(advance, initial, leading)  20.2 us
    another operation x1, loops' own time, prefix(): final_state, before = lax.scan(advance, initial, leading)  19.9 us
    all_to_all x1, starting transfers between devices, body(): lax.all_to_all(jnp.where(occupied[:, None], jnp.take(expert_input, source...  16.8 us
    all_to_all x1, starting transfers between devices, body(): lax.all_to_all(expert_rows.astype(jnp.bfloat16), EP, split_axis=0, concat...  13.6 us
  transfers between devices with their start and end apart: 5, of which 3 were waited for; matrix products, arithmetic and copies ran while one was open for 25% of the time, Pallas kernels for 0%

profile of v1, /device:TPU:1, one launch (start us, length us, event | category | flops | bytes accessed | tf_op | source)
XLA Modules:
  0.0 370.7 jit_solution(8734828979158458771)
XLA Ops:
  7.2 1.0 copy.65
  8.5 1.2 reduce-window.6
  10.9 3.9 %gather_fusion = bf16[1024,256]{1,0:T(8,128)(2,1)S(1)} fusion(bf16[256,256]{1,0:T(8,128)(2,1)S(1)} %copy-done.2, s32[1024]{0:T(1024)S(1)} %broadcast_clamp_fusion), kind=kCustom, calls=%fused_computation | custom fusion | bytes 1052672 | tf_op jit(solution)/shard_map/jit(_take)/gather | solution.py:236
  14.9 1.2 select_select_fusion
  16.0 16.8 %all-to-all-start = ((bf16[32,32,256]{2,1,0:T(8,128)(2,1)}), bf16[32,32,256]{2,1,0:T(8,128)(2,1)}, u32[]{:S(2)}, u32[]{:S(2)}) async-start(bf16[32,32,256]{2,1,0:T(8,128)(2,1)} %select_select_fusion), calls=%async_computation | async-start | bytes 1048576 | tf_op jit(solution)/shard_map/all_to_all | solution.py:233
  35.0 0.7 fusion.21
  35.8 1.4 convolution_bitcast_fusion
  37.2 65.9 %while.25 = (s32[]{:T(128)}, f32[1]{0:T(128)}, f32[1]{0:T(128)}, f32[1,128,256]{2,1,0:T(8,128)S(1)}, f32[1,128]{1,0:T(1,128)S(1)}, /*index=5*/f32[8,1]{0,1:T(1,1...) while((s32[]{:T(128)}, f32[1]{0:T(128)}, f32[1]{0:T(128)}, ...), condition=%wide.region_4.5_spmd.clone, body=%wide.region_3.4_spmd.clone.sunk | while | flops 164488 | bytes 659258 | solution.py:133
  37.2 1.3 constant_dynamic-slice_fusion.4
  41.6 0.7 fusion.105
  42.9 1.1 dynamic_update_slice.27
  44.0 1.3 dynamic_update_slice.28
  45.3 1.3 constant_dynamic-slice_fusion.4
  49.7 0.7 fusion.105
  51.0 1.2 dynamic_update_slice.27
  52.2 1.4 dynamic_update_slice.28
  53.6 1.3 constant_dynamic-slice_fusion.4
  56.7 0.7 bitcast_dynamic-update-slice_fusion.2
  58.0 0.7 fusion.105
  59.3 1.2 dynamic_update_slice.27
  60.5 1.4 dynamic_update_slice.28
  61.8 1.3 constant_dynamic-slice_fusion.4
  66.2 0.7 fusion.105
  67.5 1.2 dynamic_update_slice.27
  68.7 1.4 dynamic_update_slice.28
  70.1 1.3 constant_dynamic-slice_fusion.4
  74.5 0.7 fusion.105
  75.8 1.2 dynamic_update_slice.27
  77.0 1.4 dynamic_update_slice.28
  78.3 1.3 constant_dynamic-slice_fusion.4
  81.5 0.7 bitcast_dynamic-update-slice_fusion.2
  82.7 0.7 fusion.105
  84.0 1.2 dynamic_update_slice.27
  85.2 1.4 dynamic_update_slice.28
  86.6 1.3 constant_dynamic-slice_fusion.4
  89.7 0.7 bitcast_dynamic-update-slice_fusion.2
  91.0 0.7 fusion.105
  92.3 1.2 dynamic_update_slice.27
  93.5 1.4 dynamic_update_slice.28
  94.8 1.3 constant_dynamic-slice_fusion.4
  99.2 0.7 fusion.105
  100.5 1.2 dynamic_update_slice.27
  101.7 1.4 dynamic_update_slice.28
  103.1 2.0 all-gather.2
  111.6 0.7 maximum_bitcast_fusion.1
  112.3 5.1 %concatenate.15 = bf16[1024,16,256]{2,0,1:T(8,128)(2,1)} broadcast(bf16[1024,256]{1,0:T(8,128)(2,1)} %bitcast.133), dimensions={0,2} | broadcast | bytes 8912896 | tf_op jit(solution)/shard_map/concatenate | solution.py:17
  117.4 7.0 %all-to-all-start.1 = ((bf16[1024,16,256]{2,0,1:T(8,128)(2,1)}), bf16[1024,16,256]{2,0,1:T(8,128)(2,1)}, u32[]{:S(2)}, u32[]{:S(2)}) async-start(bf16[1024,16,256]{2,0,1:T(8,128)(2,1)} %concatenate.15), calls=%async_computation.1 | async-start | bytes 16777216 | tf_op jit(solution)/shard_map/all_to_all | solution.py:18
  125.8 52.0 %all-gather.9.cloned.1.call-done = f32[16,131,256]{2,1,0:T(8,128)} async-done(((f32[1,131,256]{2,1,0:T(8,128)}), f32[16,131,256]{2,1,0:T(8,128)}) %all-gather.9.cloned.1.call-update) | async-done | bytes 2146320 | tf_op jit(solution)/shard_map/all_gather | solution.py:38
  177.8 1.1 fusion.82
  212.4 2.0 fusion.26
  214.7 0.8 multiply_reduce_fusion.2
  215.6 0.9 fusion.17
  216.6 35.2 %all-to-all-done.1 = bf16[1024,16,256]{2,0,1:T(8,128)(2,1)} async-done(((bf16[1024,16,256]{2,0,1:T(8,128)(2,1)}), bf16[1024,16,256]{2,0,1:T(8,128)(2,1)}, u32[]{:S(2)}, u32[]{:S(2)}) %all-to-all-start.1) | async-done | bytes 8388640 | tf_op jit(solution)/shard_map/all_to_all | solution.py:18
  251.7 12.3 %copy.70 = bf16[1024,16,256]{0,2,1:T(8,128)(2,1)} copy(bf16[1024,16,256]{2,0,1:T(8,128)(2,1)} %all-to-all-done.1) | data formatting | bytes 16777216 | tf_op jit(solution)/shard_map/all_to_all | solution.py:18
  264.1 5.2 %multiply_reduce_fusion = f32[1024]{0:T(1024)S(1)} fusion(bf16[1024,16,256]{2,0,1:T(8,128)(2,1)} %all-to-all-done.1), kind=kLoop, calls=%fused_computation.12 | loop fusion | flops 12581888 | bytes 8392704 | tf_op jit(solution)/shard_map/reduce_sum | solution.py:249
  269.8 1.6 convolution_multiply_fusion.3
  271.5 1.6 fusion.8
  273.4 37.6 %all_to_all.32 = bf16[16,1024,64]{1,2,0:T(8,128)(2,1)S(1)} all-to-all(bf16[16,1024,64]{1,2,0:T(8,128)(2,1)S(1)} %broadcast_in_dim.75), channel_id=1, replica_groups=mesh['ep_0'=16,'ep_1'=2,'tp'=16] {'tp'}, dimensions={0} | all-to-all | bytes 4194304 | tf_op jit(solution)/shard_map/all_to_all | solution.py:70
  310.9 1.6 convolution_convert_fusion
  312.5 13.6 %all-to-all-start.3 = ((bf16[32,32,256]{2,1,0:T(8,128)(2,1)}), bf16[32,32,256]{2,1,0:T(8,128)(2,1)S(1)}, u32[]{:S(2)}, u32[]{:S(2)}) async-start(bf16[32,32,256]{2,1,0:T(8,128)(2,1)} %bitcast.140), calls=%async_computation.3 | async-start | bytes 1048576 | tf_op jit(solution)/shard_map/all_to_all | solution.py:257
  327.1 4.1 %convolution_convert_fusion.1 = bf16[512,256]{1,0:T(8,128)(2,1)} fusion(bf16[512,4096]{1,0:T(8,128)(2,1)} %all-gather.7.cloned.1.call-done, bf16[4096,256]{1,0:T(8,128)(2,1)S(1)} %copy-done), kind=kOutput, calls=%fused_computation.22 | convolution fusion | flops 1073872896 | bytes 6553600 | tf_op jit(solution)/shard_map/dot_general | solution.py:246
  331.2 28.4 %all-to-all-done.3 = bf16[32,32,256]{2,1,0:T(8,128)(2,1)S(1)} async-done(((bf16[32,32,256]{2,1,0:T(8,128)(2,1)}), bf16[32,32,256]{2,1,0:T(8,128)(2,1)S(1)}, u32[]{:S(2)}, u32[]{:S(2)}) %all-to-all-start.3) | async-done | bytes 524320 | tf_op jit(solution)/shard_map/all_to_all | solution.py:257
  359.6 1.9 gather_fusion.1
  361.7 2.2 multiply_reduce_fusion.1
  (148 shorter events, 17.8 us)
Async XLA Ops:
  7.2 319.9 %copy-start = (bf16[4096,256]{1,0:T(8,128)(2,1)S(1)}, bf16[4096,256]{1,0:T(8,128)(2,1)}, u32[]{:S(2)}) copy-start(bf16[4096,256]{1,0:T(8,128)(2,1)} %param.23) | copy-start | bytes 6291460
  7.2 3.7 copy-start.2
  10.9 22.0 %copy-start.15 = (f32[1,512]{1,0:T(1,128)S(1)}, f32[1,512]{1,0:T(1,128)}, u32[]{:S(2)}) copy-start(f32[1,512]{1,0:T(1,128)} %param.20) | copy-start | bytes 6148
  10.9 23.1 %copy-start.12 = (f32[1,512]{1,0:T(1,128)S(1)}, f32[1,512]{1,0:T(1,128)}, u32[]{:S(2)}) copy-start(f32[1,512]{1,0:T(1,128)} %param.19) | copy-start | bytes 6148
  14.8 20.2 %copy-start.6 = (bf16[512,128]{1,0:T(8,128)(2,1)S(1)}, bf16[512,128]{1,0:T(8,128)(2,1)}, u32[]{:S(2)}) copy-start(bf16[512,128]{1,0:T(8,128)(2,1)} %param.17) | copy-start | bytes 393220
  14.8 21.0 %copy-start.5 = (bf16[512,256]{1,0:T(8,128)(2,1)S(1)}, bf16[512,256]{1,0:T(8,128)(2,1)}, u32[]{:S(2)}) copy-start(bf16[512,256]{1,0:T(8,128)(2,1)} %param.18) | copy-start | bytes 786436
  16.0 96.3 %all-to-all-start = ((bf16[32,32,256]{2,1,0:T(8,128)(2,1)}), bf16[32,32,256]{2,1,0:T(8,128)(2,1)}, u32[]{:S(2)}, u32[]{:S(2)}) async-start(bf16[32,32,256]{2,1,0:T(8,128)(2,1)} %select_select_fusion), calls=%async_computation | async-start | bytes 1048576 | tf_op jit(solution)/shard_map/all_to_all | solution.py:233
  32.8 145.0 %all-gather.9.cloned.1.call-start = ((), (), s32[]{:S(2)}) async-start(), calls=%async_computation.5 | async-start | bytes 2367488 | tf_op jit(solution)/shard_map/all_gather | solution.py:38
  33.4 2.4 copy-start.9
  35.0 2.2 copy-start.10
  117.4 94.1 %copy-start.17 = (f32[8,1]{0,1:T(1,128)S(1)}, f32[8,1]{0,1:T(1,128)}, u32[]{:S(2)}) copy-start(f32[8,1]{0,1:T(1,128)} %get-tuple-element.76) | copy-start | bytes 100
  117.4 94.1 %copy-start.18 = (f32[8,1]{0,1:T(1,128)S(1)}, f32[8,1]{0,1:T(1,128)}, u32[]{:S(2)}) copy-start(f32[8,1]{0,1:T(1,128)} %get-tuple-element.81) | copy-start | bytes 100
  117.4 94.2 %copy-start.13 = (f32[8,1,128]{2,1,0:T(1,128)S(1)}, f32[8,1,128]{2,1,0:T(1,128)}, u32[]{:S(2)}) copy-start(f32[8,1,128]{2,1,0:T(1,128)} %get-tuple-element.83) | copy-start | bytes 12292
  117.4 94.4 %copy-start.21 = (bf16[512,128]{1,0:T(8,128)(2,1)S(1)}, bf16[512,128]{1,0:T(8,128)(2,1)}, u32[]{:S(2)}) copy-start(bf16[512,128]{1,0:T(8,128)(2,1)} %param.16) | copy-start | bytes 393220
  117.4 94.7 %copy-start.7 = (bf16[512,128]{1,0:T(8,128)(2,1)S(1)}, bf16[512,128]{1,0:T(8,128)(2,1)}, u32[]{:S(2)}) copy-start(bf16[512,128]{1,0:T(8,128)(2,1)} %param.17) | copy-start | bytes 393220
  117.4 134.3 %all-to-all-start.1 = ((bf16[1024,16,256]{2,0,1:T(8,128)(2,1)}), bf16[1024,16,256]{2,0,1:T(8,128)(2,1)}, u32[]{:S(2)}, u32[]{:S(2)}) async-start(bf16[1024,16,256]{2,0,1:T(8,128)(2,1)} %concatenate.15), calls=%async_computation.1 | async-start | bytes 16777216 | tf_op jit(solution)/shard_map/all_to_all | solution.py:18
  124.4 202.7 %all-gather.7.cloned.1.call-start = ((), (), s32[]{:S(2)}) async-start(), calls=%async_computation.4 | async-start | bytes 4456448 | tf_op jit(solution)/shard_map/all_gather | solution.py:244
  211.8 3.0 copy-start.19
  214.4 1.2 copy-start.8
  214.4 1.2 copy-start.16
  251.7 17.6 %copy-start.3 = (bf16[1,64,4096]{2,1,0:T(8,128)(2,1)S(1)}, bf16[1,64,4096]{2,1,0:T(8,128)(2,1)}, u32[]{:S(2)}) copy-start(bf16[1,64,4096]{2,1,0:T(8,128)(2,1)} %param.27) | copy-start | bytes 1572868
  264.1 5.8 %copy-start.1 = (bf16[1024,16,256]{0,2,1:T(8,128)(2,1)S(1)}, bf16[1024,16,256]{0,2,1:T(8,128)(2,1)}, u32[]{:S(2)}) copy-start(bf16[1024,16,256]{0,2,1:T(8,128)(2,1)} %copy.70) | copy-start | bytes 25165828
  269.8 1.6 copy-start.4
  273.3 37.6 %copy-start.20 = (bf16[1,1024,256]{2,1,0:T(8,128)(2,1)S(1)}, bf16[1,1024,256]{2,1,0:T(8,128)(2,1)}, u32[]{:S(2)}) copy-start(bf16[1,1024,256]{2,1,0:T(8,128)(2,1)} %param.29) | copy-start | bytes 1572868
  310.9 15.3 %copy-start.11 = (s32[256,2]{0,1:T(2,128)S(1)}, s32[256,2]{0,1:T(2,128)}, u32[]{:S(2)}) copy-start(s32[256,2]{0,1:T(2,128)} %param.25) | copy-start | bytes 6148
  310.9 15.9 %copy-start.14 = (f32[256,2]{0,1:T(2,128)S(1)}, f32[256,2]{0,1:T(2,128)}, u32[]{:S(2)}) copy-start(f32[256,2]{0,1:T(2,128)} %param.26) | copy-start | bytes 6148
  312.5 47.1 %all-to-all-start.3 = ((bf16[32,32,256]{2,1,0:T(8,128)(2,1)}), bf16[32,32,256]{2,1,0:T(8,128)(2,1)S(1)}, u32[]{:S(2)}, u32[]{:S(2)}) async-start(bf16[32,32,256]{2,1,0:T(8,128)(2,1)} %bitcast.140), calls=%async_computation.3 | async-start | bytes 1048576 | tf_op jit(solution)/shard_map/all_to_all | solution.py:257
Sparse Core Ops, SparseCore 0:
  112.4 65.3 all-gather.8
  216.7 100.4 all-gather.6
